TPU v7x, 32 devices: a whole 2x2x4 slice. The times are simulated.
32 devices in a mesh: sp: 8 (over z, y), tp: 4 (over x, core).
Axes of the slice: x: 2, y: 2, z: 4, core: 2. Of those that a mesh axis runs over, the one named last changes fastest.
Arguments:
- skip_stream_vector: bfloat16 [8192, 2048], P(('sp', 'tp')), may hold values from -6 to 6
- probe_preactivation: bfloat16 [8192, 1024], P('sp', 'tp'), may hold values from -6 to 6
- retention_preactivation: bfloat16 [8192, 1024], P('sp', 'tp'), may hold values from -4.5 to 4.5
- content_vector: bfloat16 [8192, 1024], P('sp', 'tp'), may hold values from -6 to 6
- emission_preactivation: bfloat16 [8192, 1024], P('sp', 'tp'), may hold values from -6 to 6
- retention_slack: float32 [1024], P('tp'), may hold values from 0 to 0.12
- surge_rate: float32 [8192, 1024], P('sp', 'tp'), may hold values from -1.2 to 0
- subspace_scaling_factor: float32 [1024], P('tp'), may hold values from 0.1 to 1.9
- emission_matrix: bfloat16 [1024, 2048], replicated, may hold values from -0.1875 to 0.1875
- mlp_scaling_factor: float32 [2048], replicated, may hold values from 0.1 to 1.9
- switch_matrix: bfloat16 [2048, 5632], P('sp', 'tp'), may hold values from -0.125 to 0.125
- expansion_matrix: bfloat16 [2048, 5632], P('sp', 'tp'), may hold values from -0.125 to 0.125
- contraction_matrix: bfloat16 [5632, 2048], P('tp', 'sp'), may hold values from -0.078125 to 0.078125
Outputs:
- stream_out: bfloat16 [8192, 2048], P(('sp', 'tp'))
All inputs are finite; a program needn't handle non-finite values.
Results may differ from a plain program's by a relative error of at most 0.017.
Values may be sent and summed in bfloat16 or wider, within the bound.
A program may use at most 128 MiB of HBM per device.

v0:
```python
import jax
import jax.numpy as jnp
from jax import lax
from jax.sharding import PartitionSpec as P

HEAD_DIM = 128
BLOCK = 64
EPSILON = 1e-06
TOP_PRECISION = lax.Precision.HIGHEST


def carried_in(value, axis, join, neutral):
    place = lax.axis_index(axis)
    gathered = jax.tree.map(
        lambda a, kind: lax.all_gather(a.astype(kind), axis), value, (jnp.bfloat16, jnp.bfloat16)
    )
    state = jax.tree.map(lambda a, e: jnp.zeros_like(a) + jnp.asarray(e, a.dtype), value, neutral)

    def one(turn, state):
        return join(
            state,
            jax.tree.map(
                lambda a, own: lax.dynamic_index_in_dim(a, turn, 0, False).astype(own.dtype),
                gathered,
                value,
            ),
        )

    return lax.fori_loop(0, place, one, state)


def block_step(carry, inputs):
    memory_state, offsets = carry
    query_block, input_gate_block, value_block, log_blk = inputs
    cumulative_decay = jnp.cumsum(log_blk, axis=1)
    length = log_blk.shape[1]
    carried_share = jnp.einsum(
        "eia,eax->eix",
        query_block * jnp.exp(cumulative_decay),
        memory_state,
        precision=TOP_PRECISION,
    )
    middle = cumulative_decay[:, length // 2, :][:, None, :]
    left_side = query_block * jnp.exp(cumulative_decay - middle)
    right_side = input_gate_block * jnp.exp(middle - cumulative_decay)
    causal = (jnp.arange(length)[:, None] >= jnp.arange(length)[None, :])[None, :, :]
    scores = jnp.einsum("htk,hsk->hts", left_side, right_side, precision=TOP_PRECISION)
    scores = jnp.where(causal, scores, 0.0)
    outputs = carried_share + jnp.einsum(
        "hts,hsv->htv", scores, value_block, precision=TOP_PRECISION
    )
    closing_log_decay = cumulative_decay[:, -1, :]
    updated_memory_state = jnp.exp(closing_log_decay)[:, :, None] * memory_state + jnp.einsum(
        "qnj,qnl->qjl",
        input_gate_block * jnp.exp(closing_log_decay[:, None, :] - cumulative_decay),
        value_block,
        precision=TOP_PRECISION,
    )
    return (
        (updated_memory_state, offsets + closing_log_decay),
        (outputs, cumulative_decay + offsets[:, None, :]),
    )


def split_blocks(values, heads_here):
    count = values.shape[0]
    return values.reshape(count // BLOCK, BLOCK, heads_here, HEAD_DIM).transpose(0, 2, 1, 3)


def admission_source_matrix(
    probe_preactivation, retention_preactivation, content_vector, retention_slack, surge_rate
):
    query_act = jax.nn.silu(probe_preactivation.astype(jnp.float32))
    admission_factor = retention_slack[None, :] * jax.nn.sigmoid(
        -retention_preactivation.astype(jnp.float32)
    )
    retention_logarithm = jnp.log1p(-admission_factor) + surge_rate
    return (query_act, admission_factor, content_vector.astype(jnp.float32), retention_logarithm)


def head_output(outputs, subspace_scaling_factor, emission_preactivation):
    count, heads_here = (outputs.shape[0], outputs.shape[1])
    squares = jnp.mean(outputs * outputs, axis=-1, keepdims=True)
    scaled = (
        outputs
        * lax.rsqrt(squares + EPSILON)
        * subspace_scaling_factor.reshape(heads_here, HEAD_DIM)
    )
    scaled = scaled.reshape(count, heads_here * HEAD_DIM)
    return (scaled * jax.nn.silu(emission_preactivation.astype(jnp.float32))).astype(jnp.bfloat16)


def row_norm(stream, mlp_scaling_factor):
    streamf = stream.astype(jnp.float32)
    squares = jnp.mean(streamf * streamf, axis=-1, keepdims=True)
    return (streamf * lax.rsqrt(squares + EPSILON) * mlp_scaling_factor).astype(jnp.bfloat16)


def chain(earlier, later):
    return (earlier[0] * later[0], later[0][:, :, None] * earlier[1] + later[1])


def on_device(
    skip_stream_vector,
    probe_preactivation,
    retention_preactivation,
    content_vector,
    emission_preactivation,
    retention_slack,
    surge_rate,
    subspace_scaling_factor,
    emission_matrix,
    mlp_scaling_factor,
    switch_matrix,
    expansion_matrix,
    contraction_matrix,
):
    heads_here = probe_preactivation.shape[1] // HEAD_DIM
    tok_rows = probe_preactivation.shape[0]
    arranged_sources = admission_source_matrix(
        probe_preactivation, retention_preactivation, content_vector, retention_slack, surge_rate
    )
    block_list = tuple((split_blocks(item, heads_here) for item in arranged_sources))
    start_carry = (
        jnp.zeros((heads_here, HEAD_DIM, HEAD_DIM), jnp.float32),
        jnp.zeros((heads_here, HEAD_DIM), jnp.float32),
    )
    (memory_state, offsets), (outputs, cumulative_log_decay) = lax.scan(
        block_step, start_carry, block_list
    )
    incoming_state = carried_in(
        (jnp.exp(offsets), memory_state),
        "sp",
        chain,
        (jnp.ones_like(offsets), jnp.zeros_like(memory_state)),
    )
    outputs = outputs + jnp.einsum(
        "jmxo,mos->jmxs",
        block_list[0] * jnp.exp(cumulative_log_decay),
        incoming_state[1],
        precision=TOP_PRECISION,
    )
    outputs = outputs.transpose(0, 2, 1, 3).reshape(tok_rows, heads_here, HEAD_DIM)
    mixed = head_output(outputs, subspace_scaling_factor, emission_preactivation)
    own_width = heads_here * HEAD_DIM
    own_rows = lax.dynamic_slice_in_dim(
        emission_matrix, lax.axis_index("tp") * own_width, own_width, 0
    )
    projected = lax.psum_scatter(
        jnp.dot(mixed, own_rows, preferred_element_type=jnp.float32).astype(jnp.bfloat16),
        "tp",
        scatter_dimension=0,
        tiled=True,
    ).astype(jnp.float32)
    stream = (skip_stream_vector.astype(jnp.float32) + projected).astype(jnp.bfloat16)
    normed = row_norm(stream, mlp_scaling_factor)
    all_rows = lax.all_gather(normed, "tp", axis=0, tiled=True)
    gate_proj = jnp.dot(
        all_rows,
        lax.all_gather(switch_matrix, "sp", axis=0, tiled=True),
        preferred_element_type=jnp.float32,
    )
    up_proj = jnp.dot(
        all_rows,
        lax.all_gather(expansion_matrix, "sp", axis=0, tiled=True),
        preferred_element_type=jnp.float32,
    )
    hidden = (jax.nn.silu(gate_proj) * up_proj).astype(jnp.bfloat16)
    partial_sum = jnp.dot(
        hidden,
        lax.all_gather(contraction_matrix, "sp", axis=1, tiled=True),
        preferred_element_type=jnp.float32,
    )
    summed = lax.psum_scatter(
        partial_sum.astype(jnp.bfloat16), "tp", scatter_dimension=0, tiled=True
    ).astype(jnp.float32)
    return (stream.astype(jnp.float32) + summed).astype(jnp.bfloat16)


def solution(mesh):
    in_specs = (
        P(("sp", "tp"), None),
        P("sp", "tp"),
        P("sp", "tp"),
        P("sp", "tp"),
        P("sp", "tp"),
        P("tp"),
        P("sp", "tp"),
        P("tp"),
        P(),
        P(),
        P("sp", "tp"),
        P("sp", "tp"),
        P("tp", "sp"),
    )
    out_specs = P(("sp", "tp"), None)
    return jax.shard_map(
        on_device, mesh=mesh, in_specs=in_specs, out_specs=out_specs, check_vma=False
    )
```

profile of v0, /device:TPU:0, one launch (start us, length us, event | category | flops | bytes accessed | tf_op | source)
XLA Modules:
  0.0 522.5 jit_solution(11291250167391390919)
XLA Ops:
  7.4 2.0 divide_multiply_fusion
  9.9 1.5 reshape.84
  11.4 1.3 convert_multiply_fusion.3
  13.4 2.5 reshape.90
  16.0 55.3 %while.30 = (s32[]{:T(128)}, f32[2,128,128]{2,1,0:T(8,128)S(1)}, f32[2,128]{1,0:T(2,128)S(1)}, f32[16,2,64,128]{3,2,0,1:T(8,128)}, f32[16,2,64,128]{3,2,1,0:T(8,...) while((s32[]{:T(128)}, f32[2,128,128]{2,1,0:T(8,128)S(1)}, ...), condition=%wide.region_2.3_spmd.clone, body=%wide.region_0.2_spmd.clone.sunk | while | flops 76820992 | bytes 2124949 | solution.py:128
  16.1 0.9 constant_dynamic-slice_fusion.6
  19.6 0.9 constant_dynamic-slice_fusion.6
  23.0 0.9 constant_dynamic-slice_fusion.6
  26.5 0.9 constant_dynamic-slice_fusion.6
  29.9 0.9 constant_dynamic-slice_fusion.6
  33.4 0.9 constant_dynamic-slice_fusion.6
  36.8 0.9 constant_dynamic-slice_fusion.6
  40.3 0.9 constant_dynamic-slice_fusion.6
  43.8 0.9 constant_dynamic-slice_fusion.6
  47.2 0.9 constant_dynamic-slice_fusion.6
  50.7 0.9 constant_dynamic-slice_fusion.6
  71.3 33.0 %all-gather.1 = bf16[16,128,128]{2,1,0:T(8,128)(2,1)S(1)} all-gather(bf16[2,128,128]{2,1,0:T(8,128)(2,1)S(1)} %convert_element_type.72), channel_id=3, replica_groups=mesh['sp'=8,'tp'=4] {'sp'}, dimensions={0}, use_global_device_ids=true | all-gather | bytes 589824 | tf_op jit(solution)/shard_map/all_gather | solution.py:15
  104.3 20.7 %all-gather.2 = bf16[8,2,128]{2,1,0:T(2,128)(2,1)S(1)} all-gather(bf16[1,2,128]{2,1,0:T(2,128)(2,1)S(1)} %fusion.44), channel_id=2, replica_groups=mesh['sp'=8,'tp'=4] {'sp'}, dimensions={0}, use_global_device_ids=true | all-gather | bytes 4608 | tf_op jit(solution)/shard_map/all_gather | solution.py:15
  125.1 2.8 multiply_reduce_fusion
  129.0 1.2 mul.112
  130.3 4.6 convolution_convert_fusion.1
  135.5 41.7 %reduce-scatter.3.cloned.1.call-done = bf16[256,2048]{1,0:T(8,128)(2,1)} async-done(((bf16[1024,2048]{1,0:T(8,128)(2,1)}), bf16[256,2048]{1,0:T(8,128)(2,1)}) %reduce-scatter.3.cloned.1.call-update) | async-done | bytes 1048592 | tf_op jit(solution)/shard_map/reduce_scatter | solution.py:149
  177.3 1.6 fusion.23
  178.9 2.6 fusion.25
  183.1 44.3 %all-gather.10.cloned.1.call-done = bf16[2048,1408]{1,0:T(8,128)(2,1)} async-done(((bf16[256,1408]{1,0:T(8,128)(2,1)}), bf16[2048,1408]{1,0:T(8,128)(2,1)}) %all-gather.10.cloned.1.call-update) | async-done | bytes 5767184 | tf_op jit(solution)/shard_map/all_gather | solution.py:160
  227.3 33.9 %all-gather.8.cloned.1.call-done = bf16[1024,2048]{1,0:T(8,128)(2,1)} async-done(((bf16[256,2048]{1,0:T(8,128)(2,1)}), bf16[1024,2048]{1,0:T(8,128)(2,1)}) %all-gather.8.cloned.1.call-update) | async-done | bytes 4194320 | tf_op jit(solution)/shard_map/all_gather | solution.py:157
  261.3 11.7 %fusion.49 = f32[1024,1408]{1,0:T(8,128)} fusion(bf16[1024,2048]{1,0:T(8,128)(2,1)} %all-gather.8.cloned.1.call-done, bf16[2048,1408]{1,0:T(8,128)(2,1)} %all-gather.10.cloned.1.call-done), kind=kOutput, calls=%fused_computation.85 | convolution fusion | flops 5905580032 | bytes 15728640 | tf_op jit(solution)/shard_map/dot_general | solution.py:158
  272.9 82.5 %all-gather.12.cloned.1.call-done = bf16[2048,1408]{1,0:T(8,128)(2,1)} async-done(((bf16[256,1408]{1,0:T(8,128)(2,1)}), bf16[2048,1408]{1,0:T(8,128)(2,1)}) %all-gather.12.cloned.1.call-update) | async-done | bytes 5767184 | tf_op jit(solution)/shard_map/all_gather | solution.py:165
  355.5 93.1 %all-gather.14.cloned.1.call-done = bf16[1408,2048]{1,0:T(8,128)(2,1)} async-done(((bf16[1408,256]{1,0:T(8,128)(2,1)}), bf16[1408,2048]{1,0:T(8,128)(2,1)}) %all-gather.14.cloned.1.call-update) | async-done | bytes 5767184 | tf_op jit(solution)/shard_map/all_gather | solution.py:171
  448.6 20.6 %convolution_convert_fusion = bf16[1024,2048]{1,0:T(8,128)(2,1)} fusion(bf16[1408,2048]{1,0:T(8,128)(2,1)} %all-gather.14.cloned.1.call-done, f32[1024,1408]{1,0:T(8,128)} %fusion.49, bf16[1024,2048]{1,0:T(8,128)(2,1)} %all-gather.8.cloned.1.call-done, bf16[2048,1408]{1,0:T(8,128)(2,1)} %all-gather.12.cloned.1.call-done), kind=kOutput, calls=%fused_computation.40 | convolution fusion | flops 11821907968 | bytes 25690112 | tf_op jit(solution)/shard_map/dot_general | solution.py:169
  469.2 42.9 %reduce-scatter.5.cloned.1.call-done = bf16[256,2048]{1,0:T(8,128)(2,1)} async-done(((bf16[1024,2048]{1,0:T(8,128)(2,1)}), bf16[256,2048]{1,0:T(8,128)(2,1)}) %reduce-scatter.5.cloned.1.call-update) | async-done | bytes 1048592 | tf_op jit(solution)/shard_map/reduce_scatter | solution.py:174
  512.1 2.8 fusion.26
  (218 shorter events, 48.9 us)
Async XLA Ops:
  7.4 169.9 %reduce-scatter.3.cloned.1.call-start = ((), (), s32[]{:S(2)}) async-start(), calls=%async_computation.2 | async-start | bytes 5242880 | tf_op jit(solution)/shard_map/reduce_scatter | solution.py:149
  125.0 5.2 copy-start.3
  125.0 5.2 copy-start.4
  134.9 42.4 %copy-start = (bf16[256,2048]{1,0:T(8,128)(2,1)S(1)}, bf16[256,2048]{1,0:T(8,128)(2,1)}, u32[]{:S(2)}) copy-start(bf16[256,2048]{1,0:T(8,128)(2,1)} %param.17) | copy-start | bytes 3145732
  134.9 44.0 %copy-start.2 = (f32[2048]{0:T(1024)S(1)}, f32[2048]{0:T(1024)}, u32[]{:S(2)}) copy-start(f32[2048]{0:T(1024)} %param.26) | copy-start | bytes 24580
  134.9 92.4 %all-gather.10.cloned.1.call-start = ((), (), s32[]{:S(2)}) async-start(), calls=%async_computation.4 | async-start | bytes 6488064 | tf_op jit(solution)/shard_map/all_gather | solution.py:160
  135.5 125.8 %all-gather.8.cloned.1.call-start = ((), (), s32[]{:S(2)}) async-start(), calls=%async_computation.3 | async-start | bytes 5242880 | tf_op jit(solution)/shard_map/all_gather | solution.py:157
  181.5 174.0 %all-gather.12.cloned.1.call-start = ((), (), s32[]{:S(2)}) async-start(), calls=%async_computation.5 | async-start | bytes 6488064 | tf_op jit(solution)/shard_map/all_gather | solution.py:165
  182.1 266.5 %all-gather.14.cloned.1.call-start = ((), (), s32[]{:S(2)}) async-start(), calls=%async_computation.6 | async-start | bytes 6488064 | tf_op jit(solution)/shard_map/all_gather | solution.py:171
  182.8 329.3 %reduce-scatter.5.cloned.1.call-start = ((), (), s32[]{:S(2)}) async-start(), calls=%async_computation.7 | async-start | bytes 5242880 | tf_op jit(solution)/shard_map/reduce_scatter | solution.py:174
  469.2 42.9 %copy-start.1 = (bf16[256,2048]{1,0:T(8,128)(2,1)S(1)}, bf16[256,2048]{1,0:T(8,128)(2,1)}, u32[]{:S(2)}) copy-start(bf16[256,2048]{1,0:T(8,128)(2,1)} %reduce-scatter.3.cloned.1.call-done) | copy-start | bytes 3145732
Sparse Core Ops, SparseCore 0:
  135.0 42.1 reduce-scatter.2
  469.3 42.7 reduce-scatter.4
Sparse Core Ops, SparseCore 1:
  137.6 89.7 all-gather.9
  228.8 32.4 all-gather.7
  263.3 92.1 all-gather.11
  357.5 91.0 all-gather.13
where the time goes:
time: 524 us; the launch traced here: 522 us
  waiting for transfers between devices  340 us (65%)
  matrix products  67.3 us (13%)
  blocking collectives  53.7 us (10%)
  other arithmetic  22.3 us (4%)
  local copies, waits for them, and re-layouts  22.2 us (4%)
  between operations  15.2 us (3%)
    all_gather x1, waiting for transfers between devices, on_device(): lax.all_gather(contraction_matrix, 'sp', axis=1, tiled=True)  93.1 us
    all_gather x1, waiting for transfers between devices, on_device(): lax.all_gather(expansion_matrix, 'sp', axis=0, tiled=True)  82.5 us
    all_gather x2, blocking collectives, carried_in(): lax.all_gather(a.astype(kind), axis)  53.7 us
    all_gather x1, waiting for transfers between devices, on_device(): lax.all_gather(switch_matrix, 'sp', axis=0, tiled=True)  44.3 us
    reduce_scatter x1, waiting for transfers between devices, on_device(): lax.psum_scatter(partial_sum.astype(jnp.bfloat16), 'tp', scatter_dimensio...  42.9 us
    reduce_scatter x1, waiting for transfers between devices, on_device(): lax.psum_scatter(jnp.dot(mixed, own_rows, preferred_element_type=jnp.floa...  41.7 us
    all_gather x1, waiting for transfers between devices, on_device(): all_rows = lax.all_gather(normed, 'tp', axis=0, tiled=True)  33.9 us
    dot_general x1, matrix products, on_device(): jnp.dot(hidden, lax.all_gather(contraction_matrix, 'sp', axis=1, tiled=Tr...  20.6 us
  transfers between devices with their start and end apart: 6, of which 6 were waited for; matrix products, arithmetic and copies ran while one was open for 3% of the time, Pallas kernels for 0%

commit v1 on v0

--- a/solution.py
+++ b/solution.py
@@ -154,7 +154,12 @@
     ).astype(jnp.float32)
     stream = (skip_stream_vector.astype(jnp.float32) + projected).astype(jnp.bfloat16)
     normed = row_norm(stream, mlp_scaling_factor)
-    all_rows = lax.all_gather(normed, "tp", axis=0, tiled=True)
+    ring = [normed]
+    for hop in range(3):
+        ring.append(lax.ppermute(ring[-1], "tp", [(dev, (dev + 1) % 4) for dev in range(4)]))
+    all_rows = jnp.roll(
+        jnp.concatenate(ring[::-1], axis=0), (lax.axis_index("tp") + 1) * ring[0].shape[0], axis=0
+    )
     gate_proj = jnp.dot(
         all_rows,
         lax.all_gather(switch_matrix, "sp", axis=0, tiled=True),

time: 524 us -> 488 us (0.931)
  waiting for transfers between devices: 340 us -> 292 us
  local copies, waits for them, and re-layouts: 22.2 us -> 35.7 us
    all_gather x1, waiting for transfers between devices: 44.3 us -> 0.01 us  [on_device(): lax.all_gather(switch_matrix, 'sp', axis=0, tiled=True)]
    ppermute x0 -> x3, waiting for transfers between devices: none -> 43.1 us  [on_device(): lax.ppermute(ring[-1], 'tp', [(dev, (dev + 1) % 4) for dev in range(4)])]
    all_gather x1 -> x0, waiting for transfers between devices: 33.9 us -> none  [on_device(): all_rows = lax.all_gather(normed, 'tp', axis=0, tiled=True)]
    all_gather x1, waiting for transfers between devices: 93.1 us -> 71.2 us  [on_device(): lax.all_gather(contraction_matrix, 'sp', axis=1, tiled=True)]
    unnamed x10 -> x17, local copies, waits for them, and re-layouts: 0.02 us -> 12.5 us
    all_gather x1, waiting for transfers between devices: 82.5 us -> 92.4 us  [on_device(): lax.all_gather(expansion_matrix, 'sp', axis=0, tiled=True)]
  transfers between devices with their start and end apart: 6 -> 8, of which waited for: 6 -> 7; matrix products, arithmetic and copies ran while one was open for 3% -> 6% of each run, Pallas kernels for 0% -> 0%
where the time goes in v1:
time: 488 us; the launch traced here: 487 us
  waiting for transfers between devices  292 us (60%)
  matrix products  67.3 us (14%)
  blocking collectives  53.8 us (11%)
  local copies, waits for them, and re-layouts  35.7 us (7%)
  other arithmetic  21.3 us (4%)
  between operations  15.2 us (3%)
    all_gather x1, waiting for transfers between devices, on_device(): lax.all_gather(expansion_matrix, 'sp', axis=0, tiled=True)  92.4 us
    all_gather x1, waiting for transfers between devices, on_device(): lax.all_gather(contraction_matrix, 'sp', axis=1, tiled=True)  71.2 us
    all_gather x2, blocking collectives, carried_in(): lax.all_gather(a.astype(kind), axis)  53.8 us
    ppermute x3, waiting for transfers between devices, on_device(): lax.ppermute(ring[-1], 'tp', [(dev, (dev + 1) % 4) for dev in range(4)])  43.1 us
    reduce_scatter x1, waiting for transfers between devices, on_device(): lax.psum_scatter(partial_sum.astype(jnp.bfloat16), 'tp', scatter_dimensio...  42.9 us
    reduce_scatter x1, waiting for transfers between devices, on_device(): lax.psum_scatter(jnp.dot(mixed, own_rows, preferred_element_type=jnp.floa...  40.5 us
    dot_general x1, matrix products, on_device(): jnp.dot(hidden, lax.all_gather(contraction_matrix, 'sp', axis=1, tiled=Tr...  20.6 us
    dynamic_slice x48, local copies, waits for them, and re-layouts, on_device(): lax.scan(block_step, start_carry, block_list)  14.5 us
  transfers between devices with their start and end apart: 8, of which 7 were waited for; matrix products, arithmetic and copies ran while one was open for 6% of the time, Pallas kernels for 0%

profile of v1, /device:TPU:0, one launch (start us, length us, event | category | flops | bytes accessed | tf_op | source)
XLA Modules:
  0.0 486.5 jit_solution(2251178130423047640)
XLA Ops:
  7.4 2.0 divide_multiply_fusion
  9.9 1.5 reshape.84
  11.4 1.3 convert_multiply_fusion.3
  13.4 2.6 reshape.90
  16.0 55.3 %while.30 = (s32[]{:T(128)}, f32[2,128,128]{2,1,0:T(8,128)S(1)}, f32[2,128]{1,0:T(2,128)S(1)}, f32[16,2,64,128]{3,2,0,1:T(8,128)}, f32[16,2,64,128]{3,2,1,0:T(8,...) while((s32[]{:T(128)}, f32[2,128,128]{2,1,0:T(8,128)S(1)}, ...), condition=%wide.region_2.3_spmd.clone, body=%wide.region_0.2_spmd.clone.sunk | while | flops 76820992 | bytes 2124949 | solution.py:128
  16.1 0.9 constant_dynamic-slice_fusion.6
  19.6 0.9 constant_dynamic-slice_fusion.6
  71.3 33.2 %all-gather.1 = bf16[16,128,128]{2,1,0:T(8,128)(2,1)S(1)} all-gather(bf16[2,128,128]{2,1,0:T(8,128)(2,1)S(1)} %convert_element_type.72), channel_id=3, replica_groups=mesh['sp'=8,'tp'=4] {'sp'}, dimensions={0}, use_global_device_ids=true | all-gather | bytes 589824 | tf_op jit(solution)/shard_map/all_gather | solution.py:15
  104.5 20.7 %all-gather.2 = bf16[8,2,128]{2,1,0:T(2,128)(2,1)S(1)} all-gather(bf16[1,2,128]{2,1,0:T(2,128)(2,1)S(1)} %fusion.50), channel_id=2, replica_groups=mesh['sp'=8,'tp'=4] {'sp'}, dimensions={0}, use_global_device_ids=true | all-gather | bytes 4608 | tf_op jit(solution)/shard_map/all_gather | solution.py:15
  125.2 2.8 multiply_reduce_fusion
  129.1 1.2 mul.115
  130.3 4.6 convolution_convert_fusion.1
  136.7 40.5 %reduce-scatter.3.cloned.1.call-done = bf16[256,2048]{1,0:T(8,128)(2,1)} async-done(((bf16[1024,2048]{1,0:T(8,128)(2,1)}), bf16[256,2048]{1,0:T(8,128)(2,1)}) %reduce-scatter.3.cloned.1.call-update) | async-done | bytes 1048592 | tf_op jit(solution)/shard_map/reduce_scatter | solution.py:149
  177.3 1.6 fusion.29
  178.9 1.7 fusion.31
  180.7 14.2 %collective-permute-done = bf16[256,2048]{1,0:T(8,128)(2,1)S(1)} collective-permute-done((bf16[256,2048]{1,0:T(8,128)(2,1)S(1)}, bf16[256,2048]{1,0:T(8,128)(2,1)S(1)}, u32[]{:S(2)}, u32[]{:S(2)}) %collective-permute-start) | collective-permute-done | bytes 1048608 | tf_op jit(solution)/shard_map/ppermute | solution.py:159
  194.9 14.3 %collective-permute-done.1 = bf16[256,2048]{1,0:T(8,128)(2,1)} collective-permute-done((bf16[256,2048]{1,0:T(8,128)(2,1)S(1)}, bf16[256,2048]{1,0:T(8,128)(2,1)}, u32[]{:S(2)}, u32[]{:S(2)}) %collective-permute-start.1) | collective-permute-done | bytes 1048608 | tf_op jit(solution)/shard_map/ppermute | solution.py:159
  209.2 14.5 %collective-permute-done.2 = bf16[256,2048]{1,0:T(8,128)(2,1)} collective-permute-done((bf16[256,2048]{1,0:T(8,128)(2,1)}, bf16[256,2048]{1,0:T(8,128)(2,1)}, u32[]{:S(2)}, u32[]{:S(2)}) %collective-permute-start.2) | collective-permute-done | bytes 1048608 | tf_op jit(solution)/shard_map/ppermute | solution.py:159
  223.8 2.3 constant_dynamic-update-slice_fusion.7
  226.1 2.3 constant_dynamic-update-slice_fusion.6
  228.4 1.0 constant_dynamic-update-slice_fusion.5
  229.5 1.1 constant_dynamic-update-slice_fusion.4
  230.5 2.3 constant_dynamic-update-slice_fusion.3
  232.8 2.3 constant_dynamic-update-slice_fusion.2
  235.2 1.1 constant_dynamic-update-slice_fusion.1
  236.2 1.1 constant_dynamic-update-slice_fusion
  237.3 11.7 %fusion.25 = f32[1024,1408]{1,0:T(8,128)} fusion(bf16[2048,1408]{1,0:T(8,128)(2,1)} %all-gather.7.cloned.1.call-done, bf16[2048,2048]{1,0:T(8,128)(2,1)} %constant_dynamic-update-slice_fusion, s32[]{:T(128)S(6)} %select_n.29), kind=kOutput, calls=%fused_computation.44 | convolution fusion | flops 5905580032 | bytes 15728644 | tf_op jit(solution)/shard_map/dot_general | solution.py:163
  249.1 71.2 %all-gather.11.cloned.1.call-done = bf16[1408,2048]{1,0:T(8,128)(2,1)} async-done(((bf16[1408,256]{1,0:T(8,128)(2,1)}), bf16[1408,2048]{1,0:T(8,128)(2,1)}) %all-gather.11.cloned.1.call-update) | async-done | bytes 5767184 | tf_op jit(solution)/shard_map/all_gather | solution.py:176
  320.3 92.4 %all-gather.9.cloned.1.call-done = bf16[2048,1408]{1,0:T(8,128)(2,1)} async-done(((bf16[256,1408]{1,0:T(8,128)(2,1)}), bf16[2048,1408]{1,0:T(8,128)(2,1)}) %all-gather.9.cloned.1.call-update) | async-done | bytes 5767184 | tf_op jit(solution)/shard_map/all_gather | solution.py:170
  412.7 20.6 %convolution_convert_fusion = bf16[1024,2048]{1,0:T(8,128)(2,1)} fusion(bf16[1408,2048]{1,0:T(8,128)(2,1)} %all-gather.11.cloned.1.call-done, f32[1024,1408]{1,0:T(8,128)} %fusion.25, bf16[2048,1408]{1,0:T(8,128)(2,1)} %all-gather.9.cloned.1.call-done, bf16[2048,2048]{1,0:T(8,128)(2,1)} %constant_dynamic-update-slice_fusion, s32[]{:T(128)S(6)} %select_n.29), kind=kOutput, calls=%fused_computation.40 | convolution fusion | flops 11821907968 | bytes 25690116 | tf_op jit(solution)/shard_map/dot_general | solution.py:174
  433.4 42.9 %reduce-scatter.5.cloned.1.call-done = bf16[256,2048]{1,0:T(8,128)(2,1)} async-done(((bf16[1024,2048]{1,0:T(8,128)(2,1)}), bf16[256,2048]{1,0:T(8,128)(2,1)}) %reduce-scatter.5.cloned.1.call-update) | async-done | bytes 1048592 | tf_op jit(solution)/shard_map/reduce_scatter | solution.py:179
  476.2 2.7 fusion.32
  (229 shorter events, 56.5 us)
Async XLA Ops:
  7.4 169.9 %reduce-scatter.3.cloned.1.call-start = ((), (), s32[]{:S(2)}) async-start(), calls=%async_computation.2 | async-start | bytes 5242880 | tf_op jit(solution)/shard_map/reduce_scatter | solution.py:149
  71.3 59.0 %copy-start.3 = (bf16[1024,256]{1,0:T(8,128)(2,1)S(1)}, bf16[1024,256]{1,0:T(8,128)(2,1)}, u32[]{:S(2)}) copy-start(bf16[1024,256]{1,0:T(8,128)(2,1)} %param.21) | copy-start | bytes 1572868
  71.3 59.0 %copy-start.4 = (f32[256]{0:T(256)S(1)}, f32[256]{0:T(256)}, u32[]{:S(2)}) copy-start(f32[256]{0:T(256)} %param.24) | copy-start | bytes 3076
  134.9 42.4 %copy-start = (bf16[256,2048]{1,0:T(8,128)(2,1)S(1)}, bf16[256,2048]{1,0:T(8,128)(2,1)}, u32[]{:S(2)}) copy-start(bf16[256,2048]{1,0:T(8,128)(2,1)} %param.17) | copy-start | bytes 3145732
  134.9 44.0 %copy-start.2 = (f32[2048]{0:T(1024)S(1)}, f32[2048]{0:T(1024)}, u32[]{:S(2)}) copy-start(f32[2048]{0:T(1024)} %param.26) | copy-start | bytes 24580
  134.9 102.4 %all-gather.7.cloned.1.call-start = ((), (), s32[]{:S(2)}) async-start(), calls=%async_computation.3 | async-start | bytes 6488064 | tf_op jit(solution)/shard_map/all_gather | solution.py:165
  135.5 184.8 %all-gather.11.cloned.1.call-start = ((), (), s32[]{:S(2)}) async-start(), calls=%async_computation.5 | async-start | bytes 6488064 | tf_op jit(solution)/shard_map/all_gather | solution.py:176
  136.1 276.6 %all-gather.9.cloned.1.call-start = ((), (), s32[]{:S(2)}) async-start(), calls=%async_computation.4 | async-start | bytes 6488064 | tf_op jit(solution)/shard_map/all_gather | solution.py:170
  136.7 339.6 %reduce-scatter.5.cloned.1.call-start = ((), (), s32[]{:S(2)}) async-start(), calls=%async_computation.6 | async-start | bytes 5242880 | tf_op jit(solution)/shard_map/reduce_scatter | solution.py:179
  180.6 14.3 %collective-permute-start = (bf16[256,2048]{1,0:T(8,128)(2,1)S(1)}, bf16[256,2048]{1,0:T(8,128)(2,1)S(1)}, u32[]{:S(2)}, u32[]{:S(2)}) collective-permute-start(bf16[256,2048]{1,0:T(8,128)(2,1)S(1)} %fusion.31), channel_id=1, source_target_pairs={{0,1},{1,2},{2,3},{3,0},{4,5},{5,6},{6,7},{7,4},{8,9},{9,10},{10,1... | collective-permute-start | bytes 3145736 | tf_op jit(solution)/shard_map/ppermute | solution.py:159
  194.9 14.3 %collective-permute-start.1 = (bf16[256,2048]{1,0:T(8,128)(2,1)S(1)}, bf16[256,2048]{1,0:T(8,128)(2,1)}, u32[]{:S(2)}, u32[]{:S(2)}) collective-permute-start(bf16[256,2048]{1,0:T(8,128)(2,1)S(1)} %collective-permute-done), channel_id=1, source_target_pairs={{0,1},{1,2},{2,3},{3,0},{4,5},{5,6},{6,7},{7,4},{8,9},{9,10},{10,1... | collective-permute-start | bytes 3145736 | tf_op jit(solution)/shard_map/ppermute | solution.py:159
  209.2 14.5 %collective-permute-start.2 = (bf16[256,2048]{1,0:T(8,128)(2,1)}, bf16[256,2048]{1,0:T(8,128)(2,1)}, u32[]{:S(2)}, u32[]{:S(2)}) collective-permute-start(bf16[256,2048]{1,0:T(8,128)(2,1)} %collective-permute-done.1), channel_id=1, source_target_pairs={{0,1},{1,2},{2,3},{3,0},{4,5},{5,6},{6,7},{7,4},{8,9},{9,10},{10,1... | collective-permute-start | bytes 3145736 | tf_op jit(solution)/shard_map/ppermute | solution.py:159
  249.1 227.2 %copy-start.1 = (bf16[256,2048]{1,0:T(8,128)(2,1)S(1)}, bf16[256,2048]{1,0:T(8,128)(2,1)}, u32[]{:S(2)}) copy-start(bf16[256,2048]{1,0:T(8,128)(2,1)} %reduce-scatter.3.cloned.1.call-done) | copy-start | bytes 3145732
Sparse Core Ops, SparseCore 0:
  135.0 42.1 reduce-scatter.2
  433.5 42.7 reduce-scatter.4
Sparse Core Ops, SparseCore 1:
  137.6 89.7 all-gather.6
  229.3 91.0 all-gather.10
  322.4 90.3 all-gather.8
